TPU v7x, 256 devices: a whole 4x4x8 slice. The times are simulated.
256 devices in a mesh: fs: 32 (over z, y), tp: 8 (over x, core).
Axes of the slice: x: 4, y: 4, z: 8, core: 2. Of those that a mesh axis runs over, the one named last changes fastest.
Arguments:
- prompt: bfloat16 [32768, 2048], P(('fs', 'tp')), may hold values from -6 to 6
- norm_gain: float32 [2048], P('fs'), may hold values from 0.1 to 1.9
- up_trained: float32 [2048, 8192], P('fs', 'tp'), may hold values from -0.125 to 0.125
- down_trained: float32 [2048, 8192], P('fs', 'tp'), may hold values from -0.0625 to 0.0625
Outputs:
- up_served: bfloat16 [2048, 8192], P(None, 'tp')
- down_served: bfloat16 [8192, 2048], P('tp')
- mixed: bfloat16 [32768, 2048], P(('fs', 'tp'))
All inputs are finite; a program needn't handle non-finite values.
Results may differ from a plain program's by a relative error of at most 0.014.
Values may be sent and summed in bfloat16 or wider, within the bound.
No kernel may reach another device: no remote copies, remote signals or barrier semaphores. Data moves between devices by JAX's collectives and lax.ppermute only.
A program may use at most 128 MiB of HBM per device.

v0:
```python
import jax
import jax.numpy as jnp
from jax import lax
from jax.sharding import PartitionSpec as P


def sent_together(arrays, axis, dim, along):
    both = jnp.concatenate(arrays, axis=along)
    filled, at, finished = (lax.all_gather(both, axis, axis=dim, tiled=True), 0, [])
    for a in arrays:
        finished.append(lax.slice_in_dim(filled, at, at + a.shape[along], axis=along))
        at += a.shape[along]
    return tuple(finished)


def shards(prompt, norm_gain, up_trained, down_trained):
    up_local = (norm_gain[:, None] * up_trained).astype(jnp.bfloat16)
    down_local = down_trained.astype(jnp.bfloat16)
    values = prompt.astype(jnp.float32)
    scale = lax.rsqrt(jnp.mean(values * values, axis=-1, keepdims=True) + 1e-06)
    normed = (values * scale).astype(jnp.bfloat16)
    group_rows = lax.all_gather(normed, "tp", axis=0, tiled=True)
    up_whole, down_whole = sent_together((up_local, down_local), "fs", 0, 1)
    pre = jnp.dot(group_rows, up_whole, preferred_element_type=jnp.float32)
    hidden = jnp.square(jax.nn.relu(pre)).astype(jnp.bfloat16)
    down_served = jnp.transpose(down_whole)
    mixed = lax.psum_scatter(
        jnp.dot(hidden, down_served, preferred_element_type=jnp.float32).astype(jnp.bfloat16),
        "tp",
        scatter_dimension=0,
        tiled=True,
    )
    return (up_whole, down_served, mixed)


def solution(mesh):
    return jax.shard_map(
        shards,
        mesh=mesh,
        in_specs=(P(("fs", "tp"), None), P("fs"), P("fs", "tp"), P("fs", "tp")),
        out_specs=(P(None, "tp"), P("tp", None), P(("fs", "tp"), None)),
        check_vma=False,
    )
```

profile of v0, /device:TPU:8, one launch (start us, length us, event | category | flops | bytes accessed | tf_op | source)
XLA Modules:
  0.0 207.6 jit_solution(5565873400041753207)
XLA Ops:
  7.2 0.0 all-gather.3.cloned.1.call-start
  7.2 1.0 convert_element_type.19
  8.2 1.0 multiply_convert_fusion.1
  9.2 0.7 pad_maximum_fusion
  9.9 0.0 all-gather.3.cloned.1.call-update
  10.0 0.0 all-gather.5.cloned.1.call-start
  10.0 1.2 fusion.1
  11.3 2.0 fusion.2
  13.2 0.0 all-gather.5.cloned.1.call-update
  13.3 0.0 reduce-scatter.2.cloned.1.call-start
  13.3 97.3 %all-gather.3.cloned.1.call-done = bf16[2048,2048]{1,0:T(8,128)(2,1)} async-done(((bf16[64,2048]{1,0:T(8,128)(2,1)}), bf16[2048,2048]{1,0:T(8,128)(2,1)}) %all-gather.3.cloned.1.call-update) | async-done | bytes 8388624 | tf_op jit(solution)/shard_map/all_gather | solution.py:9
  110.7 6.0 %slice_bitcast_fusion = (bf16[1024,2048]{0,1:T(8,128)(2,1)}, bf16[2048,1024]{1,0:T(8,128)(2,1)}) fusion(bf16[2048,2048]{1,0:T(8,128)(2,1)} %all-gather.3.cloned.1.call-done), kind=kLoop, calls=%fused_computation.3 | loop fusion | bytes 16777216 | tf_op jit(solution)/shard_map/transpose | solution.py:26
  116.7 29.4 %all-gather.5.cloned.1.call-done = bf16[1024,2048]{1,0:T(8,128)(2,1)} async-done(((bf16[128,2048]{1,0:T(8,128)(2,1)}), bf16[1024,2048]{1,0:T(8,128)(2,1)}) %all-gather.5.cloned.1.call-update) | async-done | bytes 4194320 | tf_op jit(solution)/shard_map/all_gather | solution.py:22
  146.0 14.4 %convolution_convert_fusion = bf16[1024,2048]{1,0:T(8,128)(2,1)} fusion(bf16[2048,2048]{1,0:T(8,128)(2,1)} %all-gather.3.cloned.1.call-done, bf16[1024,2048]{1,0:T(8,128)(2,1)} %all-gather.5.cloned.1.call-done, bf16[2048,1024]{1,0:T(8,128)(2,1)} %get-tuple-element.10), kind=kOutput, calls=%fused_computation.1 | convolution fusion | flops 8595177472 | bytes 16777216 | tf_op jit(solution)/shard_map/dot_general | solution.py:28
  160.4 0.0 reduce-scatter.2.cloned.1.call-update
  160.4 6.4 %copy.10 = bf16[1024,2048]{1,0:T(8,128)(2,1)} copy(bf16[1024,2048]{0,1:T(8,128)(2,1)} %get-tuple-element.9) | data formatting | bytes 8388608
  166.9 34.2 %reduce-scatter.2.cloned.1.call-done = bf16[128,2048]{1,0:T(8,128)(2,1)} async-done(((bf16[1024,2048]{1,0:T(8,128)(2,1)}), bf16[128,2048]{1,0:T(8,128)(2,1)}) %reduce-scatter.2.cloned.1.call-update) | async-done | bytes 524304 | tf_op jit(solution)/shard_map/reduce_scatter | solution.py:27
  (1 shorter events, 0.0 us)
Async XLA Ops:
  7.2 103.5 %all-gather.3.cloned.1.call-start = ((), (), s32[]{:S(2)}) async-start(), calls=%async_computation.1 | async-start | bytes 8650752 | tf_op jit(solution)/shard_map/all_gather | solution.py:9
  10.0 136.1 %all-gather.5.cloned.1.call-start = ((), (), s32[]{:S(2)}) async-start(), calls=%async_computation.2 | async-start | bytes 4718592 | tf_op jit(solution)/shard_map/all_gather | solution.py:22
  13.3 187.8 %reduce-scatter.2.cloned.1.call-start = ((), (), s32[]{:S(2)}) async-start(), calls=%async_computation.3 | async-start | bytes 4718592 | tf_op jit(solution)/shard_map/reduce_scatter | solution.py:27
Sparse Core Ops, SparseCore 0:
  11.1 99.4 all-gather.2
  113.1 32.8 all-gather.4
  160.5 40.4 reduce-scatter.1
where the time goes:
time: 208 us
  waiting for transfers between devices  161 us (77%)
  matrix products  14.4 us (7%)
  between operations  13.8 us (7%)
  local copies, waits for them, and re-layouts  12.5 us (6%)
  other arithmetic  5.96 us (3%)
    all_gather x1, waiting for transfers between devices, sent_together(): lax.all_gather(both, axis, axis=dim, tiled=True)  97.3 us
    reduce_scatter x1, waiting for transfers between devices, shards(): lax.psum_scatter(jnp.dot(hidden, down_served, preferred_element_type=jnp....  34.2 us
    all_gather x1, waiting for transfers between devices, shards(): group_rows = lax.all_gather(normed, 'tp', axis=0, tiled=True)  29.4 us
    dot_general x1, matrix products, shards(): jnp.dot(hidden, down_served, preferred_element_type=jnp.float32)  14.4 us
    unnamed x1, local copies, waits for them, and re-layouts  6.43 us
    transpose x1, local copies, waits for them, and re-layouts, shards(): down_served = jnp.transpose(down_whole)  6.02 us
  transfers between devices with their start and end apart: 3, of which 3 were waited for; matrix products, arithmetic and copies ran while one was open for 8% of the time, Pallas kernels for 0%

commit v1 on v0

--- a/solution.py
+++ b/solution.py
@@ -2,6 +2,12 @@
 import jax.numpy as jnp
 from jax import lax
 from jax.sharding import PartitionSpec as P
+
+
+def laid_out(blocks, dim):
+    dims = list(blocks.shape[1:])
+    dims[dim] *= blocks.shape[0]
+    return jnp.moveaxis(blocks, 0, dim).reshape(dims)
 
 
 def sent_together(arrays, axis, dim, along):
@@ -19,7 +25,19 @@
     values = prompt.astype(jnp.float32)
     scale = lax.rsqrt(jnp.mean(values * values, axis=-1, keepdims=True) + 1e-06)
     normed = (values * scale).astype(jnp.bfloat16)
-    group_rows = lax.all_gather(normed, "tp", axis=0, tiled=True)
+    size = lax.axis_size("tp")
+    pairs = [(i, (i + 1) % size) for i in range(size)]
+    back = [(b, a_2) for a_2, b in pairs]
+    lower, upper = ([], [])
+    for step in range(size - 1):
+        if step % 2 == 0:
+            lower.append(lax.ppermute(lower[-1] if lower else normed, "tp", pairs))
+        else:
+            upper.append(lax.ppermute(upper[-1] if upper else normed, "tp", back))
+    pieces = jnp.stack([*lower[::-1], normed, *upper])
+    shift = lax.axis_index("tp") - len(lower)
+    pieces = pieces[(jnp.arange(size) - shift) % size]
+    group_rows = laid_out(pieces, 0)
     up_whole, down_whole = sent_together((up_local, down_local), "fs", 0, 1)
     pre = jnp.dot(group_rows, up_whole, preferred_element_type=jnp.float32)
     hidden = jnp.square(jax.nn.relu(pre)).astype(jnp.bfloat16)

time: 208 us -> 177 us (0.85)
  waiting for transfers between devices: 161 us -> 108 us
  local copies, waits for them, and re-layouts: 12.5 us -> 24.3 us
  starting transfers between devices: 0.12 us -> 9.48 us
    all_gather x1, waiting for transfers between devices: 97.3 us -> 46 us  [sent_together(): lax.all_gather(both, axis, axis=dim, tiled=True)]
    ppermute x0 -> x7, waiting for transfers between devices: none -> 29.9 us  [the longest x4 29.9 us: shards(): lower.append(lax.ppermute(lower[-1] if lower else normed, 'tp', pairs))]
    all_gather x1 -> x0, waiting for transfers between devices: 29.4 us -> none  [shards(): group_rows = lax.all_gather(normed, 'tp', axis=0, tiled=True)]
    ppermute x0 -> x7, starting transfers between devices: none -> 9.4 us  [the longest x3 9.38 us: shards(): upper.append(lax.ppermute(upper[-1] if upper else normed, 'tp', back))]
    unnamed x1 -> x9, local copies, waits for them, and re-layouts: 6.43 us -> 12.5 us
    gather x0 -> x1, local copies, waits for them, and re-layouts: none -> 4.93 us  [shards(): pieces = pieces[(jnp.arange(size) - shift) % size]]
  transfers between devices with their start and end apart: 3 -> 9, of which waited for: 3 -> 6; matrix products, arithmetic and copies ran while one was open for 8% -> 12% of each run, Pallas kernels for 0% -> 0%
where the time goes in v1:
time: 177 us
  waiting for transfers between devices  108 us (61%)
  local copies, waits for them, and re-layouts  24.3 us (14%)
  matrix products  14.4 us (8%)
  between operations  14.1 us (8%)
  starting transfers between devices  9.48 us (5%)
  other arithmetic  6.18 us (3%)
    all_gather x1, waiting for transfers between devices, sent_together(): lax.all_gather(both, axis, axis=dim, tiled=True)  46 us
    reduce_scatter x1, waiting for transfers between devices, shards(): lax.psum_scatter(jnp.dot(hidden, down_served, preferred_element_type=jnp....  32.5 us
    ppermute x4, waiting for transfers between devices, shards(): lower.append(lax.ppermute(lower[-1] if lower else normed, 'tp', pairs))  29.9 us
    dot_general x1, matrix products, shards(): jnp.dot(hidden, down_served, preferred_element_type=jnp.float32)  14.4 us
    unnamed x9, local copies, waits for them, and re-layouts  12.5 us
    ppermute x3, starting transfers between devices, shards(): upper.append(lax.ppermute(upper[-1] if upper else normed, 'tp', back))  9.38 us
    transpose x1, local copies, waits for them, and re-layouts, shards(): down_served = jnp.transpose(down_whole)  6.02 us
    gather x1, local copies, waits for them, and re-layouts, shards(): pieces = pieces[(jnp.arange(size) - shift) % size]  4.93 us
  transfers between devices with their start and end apart: 9, of which 6 were waited for; matrix products, arithmetic and copies ran while one was open for 12% of the time, Pallas kernels for 0%

profile of v1, /device:TPU:8, one launch (start us, length us, event | category | flops | bytes accessed | tf_op | source)
XLA Modules:
  0.0 176.8 jit_solution(523667266975837938)
XLA Ops:
  7.2 0.0 copy-start
  7.2 0.0 all-gather.2.cloned.1.call-start
  7.2 1.0 convert_element_type.19
  8.2 1.0 multiply_convert_fusion.1
  9.3 0.7 pad_maximum_fusion
  10.0 0.0 all-gather.2.cloned.1.call-update
  10.0 0.0 reduce-scatter.2.cloned.1.call-start
  10.1 1.2 fusion.1
  11.3 1.2 fusion.2
  12.5 0.0 collective-permute-start
  12.5 9.8 %collective-permute-done = bf16[128,2048]{1,0:T(8,128)(2,1)S(1)} collective-permute-done((bf16[128,2048]{1,0:T(8,128)(2,1)S(1)}, bf16[128,2048]{1,0:T(8,128)(2,1)S(1)}, u32[]{:S(2)}, u32[]{:S(2)}) %collective-permute-start) | collective-permute-done | bytes 524320 | tf_op jit(solution)/shard_map/ppermute | solution.py:34
  22.4 3.0 %collective-permute-start.4 = (bf16[128,2048]{1,0:T(8,128)(2,1)S(1)}, bf16[128,2048]{1,0:T(8,128)(2,1)S(1)}, u32[]{:S(2)}, u32[]{:S(2)}) collective-permute-start(bf16[128,2048]{1,0:T(8,128)(2,1)S(1)} %fusion.2), channel_id=1, source_target_pairs={{1,0},{2,1},{3,2},{4,3},{5,4},{6,5},{7,6},{0,7},{9,8},{10,9},{11,1... | collective-permute-start | bytes 1572872 | tf_op jit(solution)/shard_map/ppermute | solution.py:36
  25.3 6.9 %collective-permute-done.1 = bf16[128,2048]{1,0:T(8,128)(2,1)S(1)} collective-permute-done((bf16[128,2048]{1,0:T(8,128)(2,1)S(1)}, bf16[128,2048]{1,0:T(8,128)(2,1)S(1)}, u32[]{:S(2)}, u32[]{:S(2)}) %collective-permute-start.1) | collective-permute-done | bytes 524320 | tf_op jit(solution)/shard_map/ppermute | solution.py:34
  32.2 3.0 %collective-permute-start.5 = (bf16[128,2048]{1,0:T(8,128)(2,1)S(1)}, bf16[128,2048]{1,0:T(8,128)(2,1)S(1)}, u32[]{:S(2)}, u32[]{:S(2)}) collective-permute-start(bf16[128,2048]{1,0:T(8,128)(2,1)S(1)} %collective-permute-done.4), channel_id=1, source_target_pairs={{1,0},{2,1},{3,2},{4,3},{5,4},{6,5},{7,6},{0,7},{9,8},{10,9},{11,1... | collective-permute-start | bytes 1572872 | tf_op jit(solution)/shard_map/ppermute | solution.py:36
  35.2 6.8 %collective-permute-done.2 = bf16[128,2048]{1,0:T(8,128)(2,1)S(1)} collective-permute-done((bf16[128,2048]{1,0:T(8,128)(2,1)S(1)}, bf16[128,2048]{1,0:T(8,128)(2,1)S(1)}, u32[]{:S(2)}, u32[]{:S(2)}) %collective-permute-start.2) | collective-permute-done | bytes 524320 | tf_op jit(solution)/shard_map/ppermute | solution.py:34
  42.0 3.4 %collective-permute-start.6 = (bf16[128,2048]{1,0:T(8,128)(2,1)S(1)}, bf16[128,2048]{1,0:T(8,128)(2,1)S(1)}, u32[]{:S(2)}, u32[]{:S(2)}) collective-permute-start(bf16[128,2048]{1,0:T(8,128)(2,1)S(1)} %collective-permute-done.5), channel_id=1, source_target_pairs={{1,0},{2,1},{3,2},{4,3},{5,4},{6,5},{7,6},{0,7},{9,8},{10,9},{11,1... | collective-permute-start | bytes 1572872 | tf_op jit(solution)/shard_map/ppermute | solution.py:36
  45.4 6.5 %collective-permute-done.3 = bf16[128,2048]{1,0:T(8,128)(2,1)} collective-permute-done((bf16[128,2048]{1,0:T(8,128)(2,1)S(1)}, bf16[128,2048]{1,0:T(8,128)(2,1)}, u32[]{:S(2)}, u32[]{:S(2)}) %collective-permute-start.3) | collective-permute-done | bytes 524320 | tf_op jit(solution)/shard_map/ppermute | solution.py:34
  51.9 1.9 %bitcast_dynamic-update-slice_fusion.7 = bf16[8,128,2048]{2,1,0:T(8,128)(2,1)} fusion(bf16[128,2048]{1,0:T(8,128)(2,1)} %collective-permute-done.3), kind=kLoop, calls=%fused_computation.16 | loop fusion | bytes 1048576
  53.8 0.8 bitcast_dynamic-update-slice_fusion.6
  54.6 0.8 bitcast_dynamic-update-slice_fusion.5
  55.4 0.8 bitcast_dynamic-update-slice_fusion.4
  56.3 0.9 bitcast_dynamic-update-slice_fusion.3
  57.2 0.8 bitcast_dynamic-update-slice_fusion.2
  58.1 0.8 bitcast_dynamic-update-slice_fusion.1
  58.9 0.8 bitcast_dynamic-update-slice_fusion
  59.7 4.9 %gather_fusion = bf16[8,128,2048]{2,1,0:T(8,128)(2,1)} fusion(bf16[8,128,2048]{2,1,0:T(8,128)(2,1)} %bitcast_dynamic-update-slice_fusion, s32[1024]{0:T(1024)S(1)} %pad_clamp_fusion), kind=kCustom, calls=%fused_computation | custom fusion | bytes 8388640 | tf_op jit(solution)/shard_map/gather | solution.py:39
  64.7 46.0 %all-gather.2.cloned.1.call-done = bf16[2048,2048]{1,0:T(8,128)(2,1)} async-done(((bf16[64,2048]{1,0:T(8,128)(2,1)}), bf16[2048,2048]{1,0:T(8,128)(2,1)}) %all-gather.2.cloned.1.call-update) | async-done | bytes 8388624 | tf_op jit(solution)/shard_map/all_gather | solution.py:15
  110.7 6.0 %slice_bitcast_fusion = (bf16[1024,2048]{0,1:T(8,128)(2,1)}, bf16[2048,1024]{1,0:T(8,128)(2,1)}) fusion(bf16[2048,2048]{1,0:T(8,128)(2,1)} %all-gather.2.cloned.1.call-done), kind=kLoop, calls=%fused_computation.4 | loop fusion | bytes 16777216 | tf_op jit(solution)/shard_map/transpose | solution.py:44
  116.7 14.4 %convolution_convert_fusion = bf16[1024,2048]{1,0:T(8,128)(2,1)} fusion(bf16[2048,2048]{1,0:T(8,128)(2,1)} %all-gather.2.cloned.1.call-done, bf16[1024,2048]{1,0:T(8,128)(2,1)} %bitcast.23, bf16[2048,1024]{1,0:T(8,128)(2,1)} %get-tuple-element.10), kind=kOutput, calls=%fused_computation.2 | convolution fusion | flops 8595177472 | bytes 16777216 | tf_op jit(solution)/shard_map/dot_general | solution.py:46
  131.1 0.0 reduce-scatter.2.cloned.1.call-update
  131.1 6.4 %copy.10 = bf16[1024,2048]{1,0:T(8,128)(2,1)} copy(bf16[1024,2048]{0,1:T(8,128)(2,1)} %get-tuple-element.9) | data formatting | bytes 8388608
  137.5 32.5 %reduce-scatter.2.cloned.1.call-done = bf16[128,2048]{1,0:T(8,128)(2,1)} async-done(((bf16[1024,2048]{1,0:T(8,128)(2,1)}), bf16[128,2048]{1,0:T(8,128)(2,1)}) %reduce-scatter.2.cloned.1.call-update) | async-done | bytes 524304 | tf_op jit(solution)/shard_map/reduce_scatter | solution.py:45
  (10 shorter events, 0.0 us)
Async XLA Ops:
  7.2 49.1 %copy-start = (bf16[128,2048]{1,0:T(8,128)(2,1)S(1)}, bf16[128,2048]{1,0:T(8,128)(2,1)}, u32[]{:S(2)}) copy-start(bf16[128,2048]{1,0:T(8,128)(2,1)} %param.4) | copy-start | bytes 1572868
  7.2 103.5 %all-gather.2.cloned.1.call-start = ((), (), s32[]{:S(2)}) async-start(), calls=%async_computation.1 | async-start | bytes 8650752 | tf_op jit(solution)/shard_map/all_gather | solution.py:15
  10.0 160.0 %reduce-scatter.2.cloned.1.call-start = ((), (), s32[]{:S(2)}) async-start(), calls=%async_computation.2 | async-start | bytes 4718592 | tf_op jit(solution)/shard_map/reduce_scatter | solution.py:45
  12.5 9.8 %collective-permute-start = (bf16[128,2048]{1,0:T(8,128)(2,1)S(1)}, bf16[128,2048]{1,0:T(8,128)(2,1)S(1)}, u32[]{:S(2)}, u32[]{:S(2)}) collective-permute-start(bf16[128,2048]{1,0:T(8,128)(2,1)S(1)} %fusion.2), channel_id=1, source_target_pairs={{0,1},{1,2},{2,3},{3,4},{4,5},{5,6},{6,7},{7,0},{8,9},{9,10},{10,1... | collective-permute-start | bytes 1572872 | tf_op jit(solution)/shard_map/ppermute | solution.py:34
  22.3 9.8 %collective-permute-start.1 = (bf16[128,2048]{1,0:T(8,128)(2,1)S(1)}, bf16[128,2048]{1,0:T(8,128)(2,1)S(1)}, u32[]{:S(2)}, u32[]{:S(2)}) collective-permute-start(bf16[128,2048]{1,0:T(8,128)(2,1)S(1)} %collective-permute-done), channel_id=1, source_target_pairs={{0,1},{1,2},{2,3},{3,4},{4,5},{5,6},{6,7},{7,0},{8,9},{9,10},{10,1... | collective-permute-start | bytes 1572872 | tf_op jit(solution)/shard_map/ppermute | solution.py:34
  22.4 9.8 %collective-permute-start.4 = (bf16[128,2048]{1,0:T(8,128)(2,1)S(1)}, bf16[128,2048]{1,0:T(8,128)(2,1)S(1)}, u32[]{:S(2)}, u32[]{:S(2)}) collective-permute-start(bf16[128,2048]{1,0:T(8,128)(2,1)S(1)} %fusion.2), channel_id=1, source_target_pairs={{1,0},{2,1},{3,2},{4,3},{5,4},{6,5},{7,6},{0,7},{9,8},{10,9},{11,1... | collective-permute-start | bytes 1572872 | tf_op jit(solution)/shard_map/ppermute | solution.py:36
  32.2 9.8 %collective-permute-start.2 = (bf16[128,2048]{1,0:T(8,128)(2,1)S(1)}, bf16[128,2048]{1,0:T(8,128)(2,1)S(1)}, u32[]{:S(2)}, u32[]{:S(2)}) collective-permute-start(bf16[128,2048]{1,0:T(8,128)(2,1)S(1)} %collective-permute-done.1), channel_id=1, source_target_pairs={{0,1},{1,2},{2,3},{3,4},{4,5},{5,6},{6,7},{7,0},{8,9},{9,10},{10,1... | collective-permute-start | bytes 1572872 | tf_op jit(solution)/shard_map/ppermute | solution.py:34
  32.2 9.8 %collective-permute-start.5 = (bf16[128,2048]{1,0:T(8,128)(2,1)S(1)}, bf16[128,2048]{1,0:T(8,128)(2,1)S(1)}, u32[]{:S(2)}, u32[]{:S(2)}) collective-permute-start(bf16[128,2048]{1,0:T(8,128)(2,1)S(1)} %collective-permute-done.4), channel_id=1, source_target_pairs={{1,0},{2,1},{3,2},{4,3},{5,4},{6,5},{7,6},{0,7},{9,8},{10,9},{11,1... | collective-permute-start | bytes 1572872 | tf_op jit(solution)/shard_map/ppermute | solution.py:36
  42.0 9.9 %collective-permute-start.3 = (bf16[128,2048]{1,0:T(8,128)(2,1)S(1)}, bf16[128,2048]{1,0:T(8,128)(2,1)}, u32[]{:S(2)}, u32[]{:S(2)}) collective-permute-start(bf16[128,2048]{1,0:T(8,128)(2,1)S(1)} %collective-permute-done.2), channel_id=1, source_target_pairs={{0,1},{1,2},{2,3},{3,4},{4,5},{5,6},{6,7},{7,0},{8,9},{9,10},{10,1... | collective-permute-start | bytes 1572872 | tf_op jit(solution)/shard_map/ppermute | solution.py:34
  42.0 16.9 %collective-permute-start.6 = (bf16[128,2048]{1,0:T(8,128)(2,1)S(1)}, bf16[128,2048]{1,0:T(8,128)(2,1)S(1)}, u32[]{:S(2)}, u32[]{:S(2)}) collective-permute-start(bf16[128,2048]{1,0:T(8,128)(2,1)S(1)} %collective-permute-done.5), channel_id=1, source_target_pairs={{1,0},{2,1},{3,2},{4,3},{5,4},{6,5},{7,6},{0,7},{9,8},{10,9},{11,1... | collective-permute-start | bytes 1572872 | tf_op jit(solution)/shard_map/ppermute | solution.py:36
Sparse Core Ops, SparseCore 0:
  11.1 99.4 all-gather.1
  131.2 38.7 reduce-scatter.1
